TPU v7x, 32 devices: a whole 2x2x4 slice. The times are simulated.
32 devices in a mesh: dp: 4 (over y, x), kv: 4 (over z), tp: 2 (over core).
Axes of the slice: x: 2, y: 2, z: 4, core: 2. Of those that a mesh axis runs over, the one named last changes fastest.
Arguments:
- tokens: bfloat16 [1024, 4096], P('dp', ('kv', 'tp')), may hold values from -53 to 53
- carried_state: float32 [1024, 16, 128, 128], P(('dp', 'kv', 'tp')), may hold values from -9 to 9
- first_gain: float32 [4096], replicated, may hold values from 0.1 to 1.9
- first_gate: bfloat16 [4096, 11264], P(None, ('kv', 'tp')), may hold values from -0.09375 to 0.09375
- first_up: bfloat16 [4096, 11264], P(None, ('kv', 'tp')), may hold values from -0.09375 to 0.09375
- first_down: bfloat16 [11264, 4096], P(('kv', 'tp')), may hold values from -0.078125 to 0.078125
- mix_gain: float32 [4096], replicated, may hold values from 0.1 to 1.9
- query_weight: bfloat16 [4096, 2048], P(('kv', 'tp')), may hold values from -0.09375 to 0.09375
- forget_weight: bfloat16 [4096, 2048], P(('kv', 'tp')), may hold values from -0.09375 to 0.09375
- input_weight: bfloat16 [4096, 2048], P(('kv', 'tp')), may hold values from -0.09375 to 0.09375
- outgate_weight: bfloat16 [4096, 2048], P(('kv', 'tp')), may hold values from -0.09375 to 0.09375
- forget_floor: float32 [2048], replicated, may hold values from 0.05 to 0.9
- head_gain: float32 [128], replicated, may hold values from 0.1 to 1.9
- output_weight: bfloat16 [2048, 4096], P(None, ('kv', 'tp')), may hold values from -0.125 to 0.125
- second_gain: float32 [4096], replicated, may hold values from 0.1 to 1.9
- second_gate: bfloat16 [4096, 11264], P(None, ('kv', 'tp')), may hold values from -0.09375 to 0.09375
- second_up: bfloat16 [4096, 11264], P(None, ('kv', 'tp')), may hold values from -0.09375 to 0.09375
- second_down: bfloat16 [11264, 4096], P(('kv', 'tp')), may hold values from -0.078125 to 0.078125
Outputs:
- layer_out: bfloat16 [1024, 4096], P('dp', ('kv', 'tp'))
- next_state: float32 [1024, 16, 128, 128], P(('dp', 'kv', 'tp'))
All inputs are finite; a program needn't handle non-finite values.
Results may differ from a plain program's by a relative error of at most 0.018.
Values may be sent and summed in bfloat16 or wider, within the bound.
A program may use at most 256 MiB of HBM per device.

v0:
```python
import functools

import jax
import jax.numpy as jnp
from jax import lax
from jax.experimental import pallas as pl
from jax.experimental.pallas import tpu as pltpu
from jax.sharding import PartitionSpec as P

epsilon = 1e-06
MESH = pl.DeviceIdType.MESH
VMEM_LIMIT = 62 * 1024 * 1024


def remote(src, dst, send_sem, recv_sem, kv, tp):
    return pltpu.make_async_remote_copy(
        src_ref=src,
        dst_ref=dst,
        send_sem=send_sem,
        recv_sem=recv_sem,
        device_id={"kv": kv, "tp": tp},
        device_id_type=MESH,
    )


def greet(me, core, chips):
    barrier = pltpu.get_barrier_semaphore()
    pl.semaphore_signal(
        barrier, inc=1, device_id={"kv": me, "tp": 1 - core}, device_id_type=MESH
    )
    for step in range(1, chips):
        pl.semaphore_signal(
            barrier,
            inc=1,
            device_id={"kv": lax.rem(me + step, chips), "tp": core},
            device_id_type=MESH,
        )
    pl.semaphore_wait(barrier, chips)


def gather_kernel(chips, own_ref, full_ref, local_sem, chip_send, sib_send, recv_sem):
    me = lax.axis_index("kv")
    core = lax.axis_index("tp")
    mine = me * 2 + core
    local = pltpu.make_async_copy(own_ref, full_ref.at[mine], local_sem)
    local.start()
    greet(me, core, chips)
    sends = []
    for step in range(1, chips):
        peer = lax.rem(me + chips - step, chips)
        copy = remote(
            own_ref, full_ref.at[mine], chip_send.at[step], recv_sem.at[mine], peer, core
        )
        copy.start()
        sends.append(copy)
    copy = remote(own_ref, full_ref.at[mine], sib_send.at[0], recv_sem.at[mine], me, 1 - core)
    copy.start()
    sends.append(copy)
    for step in range(1, chips):
        slot = lax.rem(me + step, chips) * 2 + core
        remote(
            full_ref.at[slot], full_ref.at[slot], chip_send.at[0], recv_sem.at[slot], me, 1 - core
        ).wait_recv()
        copy = remote(
            full_ref.at[slot], full_ref.at[slot], sib_send.at[step], recv_sem.at[slot], me, 1 - core
        )
        copy.start()
        sends.append(copy)
    for step in range(chips):
        slot = lax.rem(me + step, chips) * 2 + 1 - core
        remote(
            full_ref.at[slot], full_ref.at[slot], chip_send.at[0], recv_sem.at[slot], me, 1 - core
        ).wait_recv()
    for copy in sends:
        copy.wait_send()
    local.wait()


def gather_rows(own, chips, collective_id):
    blocks = chips * 2
    return pl.pallas_call(
        functools.partial(gather_kernel, chips),
        out_shape=jax.ShapeDtypeStruct((blocks,) + own.shape, own.dtype),
        in_specs=[pl.BlockSpec(memory_space=pltpu.VMEM)],
        out_specs=pl.BlockSpec(memory_space=pltpu.VMEM),
        scratch_shapes=[
            pltpu.SemaphoreType.DMA,
            pltpu.SemaphoreType.DMA((chips,)),
            pltpu.SemaphoreType.DMA((chips,)),
            pltpu.SemaphoreType.DMA((blocks,)),
        ],
        compiler_params=pltpu.CompilerParams(
            collective_id=collective_id, has_side_effects=True, vmem_limit_bytes=VMEM_LIMIT
        ),
    )(own)


def block_kernel(
    chips,
    own_ref,
    gain_ref,
    gate_hbm,
    up_hbm,
    down_hbm,
    out_ref,
    gate_w,
    up_w,
    down_w,
    cols,
    gate_acc,
    up_acc,
    squares,
    hidden,
    sib_out,
    sib_in,
    chip_out,
    chip_in,
    gate_sem,
    up_sem,
    down_sem,
    local_sem,
    chip_send,
    sib_send,
    recv_sem,
    sib_out_sem,
    sib_in_sem,
    chip_out_sem,
    chip_in_sem,
):
    me = lax.axis_index("kv")
    core = lax.axis_index("tp")
    mine = me * 2 + core
    rows, width = own_ref.shape
    full_width = width * chips * 2

    def gate_copy(j):
        at = pl.ds(pl.multiple_of(j * width, width), width)
        return pltpu.make_async_copy(gate_hbm.at[at, :], gate_w.at[j], gate_sem.at[j])

    def up_copy(j):
        at = pl.ds(pl.multiple_of(j * width, width), width)
        return pltpu.make_async_copy(up_hbm.at[at, :], up_w.at[j], up_sem.at[j])

    def down_copy(j):
        at = pl.ds(pl.multiple_of(j * width, width), width)
        return pltpu.make_async_copy(down_hbm.at[:, at], down_w.at[j], down_sem.at[j])

    local = pltpu.make_async_copy(own_ref, cols.at[mine], local_sem)
    local.start()

    @pl.loop(0, chips)
    def _(step):
        q = lax.rem(me + step, chips)
        for c in (core, 1 - core):
            gate_copy(q * 2 + c).start()
            up_copy(q * 2 + c).start()

    greet(me, core, chips)

    def share_copy(step):
        return remote(
            own_ref,
            cols.at[mine],
            chip_send.at[step],
            recv_sem.at[mine],
            lax.rem(me + chips - step, chips),
            core,
        )

    def pass_copy(slot, step):
        return remote(
            cols.at[slot], cols.at[slot], sib_send.at[step], recv_sem.at[slot], me, 1 - core
        )

    @pl.loop(1, chips)
    def _(step):
        share_copy(step).start()

    @pl.loop(0, chips)
    def _(step):
        q = lax.rem(me + 1 + step, chips)
        for c in (1 - core, core):
            down_copy(q * 2 + c).start()

    gate_acc[...] = jnp.zeros_like(gate_acc)
    up_acc[...] = jnp.zeros_like(up_acc)
    squares[...] = jnp.zeros_like(squares)
    local.wait()

    def take(j):
        block = cols[j].astype(jnp.float32)
        squares[...] += jnp.sum(block * block, axis=1, keepdims=True)
        scaled = (block * gain_ref[j]).astype(jnp.bfloat16)
        gate_copy(j).wait()
        gate_acc[...] += jnp.dot(scaled, gate_w[j], preferred_element_type=jnp.float32)
        up_copy(j).wait()
        up_acc[...] += jnp.dot(scaled, up_w[j], preferred_element_type=jnp.float32)

    @pl.loop(0, chips * 2)
    def _(turn):
        step = lax.div(turn, 2)
        other = lax.rem(turn, 2)
        q = lax.rem(me + step, chips)
        slot = q * 2 + lax.rem(core + other, 2)

        @pl.when(turn > 0)
        def _():
            pass_copy(slot, step).wait_recv()

        @pl.when(other == 0)
        def _():
            pass_copy(slot, step).start()

        take(slot)

    tile = 32

    @pl.loop(0, rows // tile)
    def _(i):
        at = pl.ds(pl.multiple_of(i * tile, tile), tile)
        row_scale = lax.rsqrt(squares[at, :] / full_width + epsilon)
        gate = row_scale * gate_acc[at, :]
        hidden[at, :] = (gate * jax.nn.sigmoid(gate) * (row_scale * up_acc[at, :])).astype(
            jnp.bfloat16
        )

    def branch(j):
        down_copy(j).wait()
        return 0.5 * jnp.dot(hidden[...], down_w[j], preferred_element_type=jnp.float32)

    def sib_copy(q):
        return remote(
            sib_out.at[q], sib_in.at[q], sib_out_sem.at[q], sib_in_sem.at[q], me, 1 - core
        )

    def chip_copy(q):
        return remote(
            chip_out.at[q], chip_in.at[me], chip_out_sem.at[q], chip_in_sem.at[me], q, core
        )

    @pl.loop(0, chips)
    def _(step):
        q = lax.rem(me + 1 + step, chips)
        sib_out[q] = branch(q * 2 + 1 - core).astype(jnp.bfloat16)
        sib_copy(q).start()
        part = branch(q * 2 + core)
        sib_copy(q).wait_recv()
        chip_out[q] = (part + sib_in[q].astype(jnp.float32)).astype(jnp.bfloat16)

        @pl.when(step < chips - 1)
        def _():
            chip_copy(q).start()

        @pl.when(step == chips - 1)
        def _():
            gate_acc[:, :width] = part + sib_in[q].astype(jnp.float32)

    total = gate_acc[:, :width] + own_ref[...].astype(jnp.float32)
    for step in range(1, chips):
        q = lax.rem(me + step, chips)
        remote(
            chip_out.at[q], chip_in.at[q], chip_out_sem.at[q], chip_in_sem.at[q], q, core
        ).wait_recv()
        total = total + chip_in[q].astype(jnp.float32)
    out_ref[...] = total.astype(out_ref.dtype)

    @pl.loop(0, chips)
    def _(step):
        slot = lax.rem(me + step, chips) * 2 + core
        pass_copy(slot, step).wait_send()
        sib_copy(step).wait_send()

    @pl.loop(1, chips)
    def _(step):
        share_copy(step).wait_send()
        chip_copy(lax.rem(me + step, chips)).wait_send()


def feed_forward(own, gain, gate, up, down, chips, collective_id):
    rows, width = own.shape
    units = gate.shape[1]
    blocks = chips * 2
    dma = pltpu.SemaphoreType.DMA
    acc_width = max(units, width)
    return pl.pallas_call(
        functools.partial(block_kernel, chips),
        out_shape=jax.ShapeDtypeStruct((rows, width), jnp.bfloat16),
        in_specs=[pl.BlockSpec(memory_space=pltpu.VMEM)] * 2
        + [pl.BlockSpec(memory_space=pl.ANY)] * 3,
        out_specs=pl.BlockSpec(memory_space=pltpu.VMEM),
        scratch_shapes=[
            pltpu.VMEM((blocks, width, units), jnp.bfloat16),
            pltpu.VMEM((blocks, width, units), jnp.bfloat16),
            pltpu.VMEM((blocks, units, width), jnp.bfloat16),
            pltpu.VMEM((blocks, rows, width), jnp.bfloat16),
            pltpu.VMEM((rows, units), jnp.float32),
            pltpu.VMEM((rows, units), jnp.float32),
            pltpu.VMEM((rows, 1), jnp.float32),
            pltpu.VMEM((rows, units), jnp.bfloat16),
            pltpu.VMEM((chips, rows, width), jnp.bfloat16),
            pltpu.VMEM((chips, rows, width), jnp.bfloat16),
            pltpu.VMEM((chips, rows, width), jnp.bfloat16),
            pltpu.VMEM((chips, rows, width), jnp.bfloat16),
            dma((blocks,)),
            dma((blocks,)),
            dma((blocks,)),
            dma,
            dma((chips,)),
            dma((chips,)),
            dma((blocks,)),
            dma((chips,)),
            dma((chips,)),
            dma((chips,)),
            dma((chips,)),
        ],
        compiler_params=pltpu.CompilerParams(
            collective_id=collective_id, has_side_effects=True, vmem_limit_bytes=VMEM_LIMIT
        ),
    )(own, gain.reshape(blocks, 1, width), gate, up, down)


def state_kernel(old_ref, forget_ref, query_ref, value_ref, new_ref, readout_ref):
    batch, heads = old_ref.shape[:2]
    for s in range(batch):
        for h in range(heads):
            value = value_ref[s, h : h + 1, :]
            new = value + forget_ref[s, :, h : h + 1] * (old_ref[s, h] - value)
            new_ref[s, h] = new
            readout_ref[s, h : h + 1, :] = jnp.sum(
                new * query_ref[s, :, h : h + 1], axis=0, keepdims=True
            )


def update_state(carried, forget, query, value):
    rows, heads, keys, values = carried.shape
    batch = 2 if rows % 2 == 0 else 1
    cells = rows * heads * keys * values
    return pl.pallas_call(
        state_kernel,
        grid=(rows // batch,),
        out_shape=(
            jax.ShapeDtypeStruct(carried.shape, jnp.float32),
            jax.ShapeDtypeStruct((rows, heads, values), jnp.float32),
        ),
        in_specs=[
            pl.BlockSpec((batch, heads, keys, values), lambda i: (i, 0, 0, 0)),
            pl.BlockSpec((batch, keys, heads), lambda i: (i, 0, 0)),
            pl.BlockSpec((batch, keys, heads), lambda i: (i, 0, 0)),
            pl.BlockSpec((batch, heads, values), lambda i: (i, 0, 0)),
        ],
        out_specs=(
            pl.BlockSpec((batch, heads, keys, values), lambda i: (i, 0, 0, 0)),
            pl.BlockSpec((batch, heads, values), lambda i: (i, 0, 0)),
        ),
        compiler_params=pltpu.CompilerParams(vmem_limit_bytes=32 * 1024 * 1024),
        cost_estimate=pl.CostEstimate(
            flops=5 * cells, bytes_accessed=8 * cells, transcendentals=0
        ),
    )(carried, forget.swapaxes(1, 2), query.swapaxes(1, 2), value)


def per_device(
    tokens,
    carried_state,
    first_gain,
    first_gate,
    first_up,
    first_down,
    mix_gain,
    query_weight,
    forget_weight,
    input_weight,
    outgate_weight,
    forget_floor,
    head_gain,
    output_weight,
    second_gain,
    second_gate,
    second_up,
    second_down,
):
    own_index = lax.axis_index(("kv", "tp"))
    group_size = lax.axis_size(("kv", "tp"))
    share_cols = tokens.shape[1]
    full_width = share_cols * group_size
    chips = lax.axis_size("kv")
    mixer_share = feed_forward(tokens, first_gain, first_gate, first_up, first_down, chips, 0)
    share_wide = mixer_share.astype(jnp.float32)
    mix_scaled = (
        share_wide * lax.dynamic_slice_in_dim(mix_gain, own_index * share_cols, share_cols)
    ).astype(jnp.bfloat16)
    state_rows, head_count, key_size, value_size = carried_state.shape
    squares = jnp.sum(share_wide * share_wide, axis=1).reshape(-1, 128)
    lines = squares.shape[0]
    padded = jnp.pad(squares, ((0, -lines % 8), (0, 0)))
    squares = jnp.sum(gather_rows(padded, chips, 3), axis=0)[:lines].reshape(-1)
    projected = lax.psum_scatter(
        jnp.concatenate(
            [
                jnp.dot(mix_scaled, weight_part, preferred_element_type=jnp.float32)
                for weight_part in (query_weight, forget_weight, input_weight, outgate_weight)
            ],
            axis=1,
        ).astype(jnp.bfloat16),
        ("kv", "tp"),
        scatter_dimension=0,
        tiled=True,
    ).astype(jnp.float32)
    own_squares = lax.dynamic_slice_in_dim(squares, own_index * state_rows, state_rows)
    projected = projected * lax.rsqrt(own_squares / full_width + epsilon)[:, None]
    key_width = head_count * key_size
    value_width = head_count * value_size
    query_act = projected[:, :key_width].reshape(state_rows, head_count, key_size)
    forget_pre = projected[:, key_width : 2 * key_width].reshape(state_rows, head_count, key_size)
    input_val = projected[:, 2 * key_width : 2 * key_width + value_width].reshape(
        state_rows, head_count, value_size
    )
    gate_pre = projected[:, 2 * key_width + value_width :].reshape(
        state_rows, head_count, value_size
    )
    floor_grid = forget_floor.reshape(head_count, key_size)
    forget = floor_grid + (1.0 - floor_grid) * jax.nn.sigmoid(forget_pre)
    next_state, readout = update_state(carried_state, forget, jax.nn.silu(query_act), input_val)
    normed = (
        readout
        * lax.rsqrt(jnp.mean(readout * readout, axis=-1, keepdims=True) + epsilon)
        * head_gain
    )
    mixer_out = (
        (normed * jax.nn.silu(gate_pre)).reshape(state_rows, value_width).astype(jnp.bfloat16)
    )
    update = jnp.dot(
        gather_rows(mixer_out, chips, 1).reshape(state_rows * group_size, value_width),
        output_weight,
        preferred_element_type=jnp.float32,
    )
    middle = (share_wide + update).astype(jnp.bfloat16)
    layer_out = feed_forward(middle, second_gain, second_gate, second_up, second_down, chips, 2)
    return (layer_out, next_state)


def solution(mesh):
    in_specs = (
        P("dp", ("kv", "tp")),
        P(("dp", "kv", "tp"), None, None, None),
        P(),
        P(None, ("kv", "tp")),
        P(None, ("kv", "tp")),
        P(("kv", "tp"), None),
        P(),
        P(("kv", "tp"), None),
        P(("kv", "tp"), None),
        P(("kv", "tp"), None),
        P(("kv", "tp"), None),
        P(),
        P(),
        P(None, ("kv", "tp")),
        P(),
        P(None, ("kv", "tp")),
        P(None, ("kv", "tp")),
        P(("kv", "tp"), None),
    )
    out_specs = (P("dp", ("kv", "tp")), P(("dp", "kv", "tp"), None, None, None))
    return jax.shard_map(
        per_device, mesh=mesh, in_specs=in_specs, out_specs=out_specs, check_vma=False
    )
```

profile of v0, /device:TPU:0, one launch (start us, length us, event | category | flops | bytes accessed | tf_op | source)
XLA Modules:
  0.0 251.5 jit_solution(15689412751257035926)
XLA Ops:
  7.2 0.0 reduce-scatter.2.cloned.1.call-start
  7.2 0.8 dynamic_slice.6
  8.0 56.5 %shard_map.185 = bf16[256,512]{1,0:T(8,128)(2,1)} custom-call(bf16[256,512]{1,0:T(8,128)(2,1)} %own_ref.1, f32[8,1,512]{2,1,0:T(1,128)} %bitcast.55, bf16[4096,1408]{1,0:T(8,128)(2,1)} %gate_hbm.2, bf16[4096,1408]{1,0:T(8,128)(2,1)} %up_hbm.2, bf16[1408,4096]{1,0:T(8,128)(2,1)} %down_hbm.2), custom_call_target="tpu_custom_call" | custom-call | tf_op jit(solution)/shard_map/pallas_call | solution.py:285
  64.5 2.5 %convolution_convert_fusion.2 = bf16[256,2048]{1,0:T(8,128)(2,1)S(1)} fusion(bf16[512,2048]{1,0:T(8,128)(2,1)} %param.26, bf16[256,512]{1,0:T(8,128)(2,1)} %shard_map.185, f32[512]{0:T(512)S(1)} %dynamic_slice.6), kind=kOutput, calls=%fused_computation.3 | convolution fusion | flops 537788416 | bytes 3409920 | tf_op jit(solution)/shard_map/dot_general | solution.py:400
  67.0 0.7 convolution_convert_fusion.1
  67.8 0.9 copy-done.2
  68.6 0.7 convolution_convert_fusion
  69.4 0.9 copy-done.3
  70.2 0.7 convolution_convert_fusion.3
  70.9 2.2 pad_maximum_fusion
  73.2 0.7 copy-done.4
  73.9 0.1 copy.36
  74.0 0.1 copy.35
  74.1 0.1 fusion.2
  74.2 0.6 pad.4.own_ref
  74.8 11.7 %shard_map.186 = f32[8,8,128]{2,1,0:T(8,128)} custom-call(f32[8,128]{1,0:T(8,128)} %pad.4.own_ref), custom_call_target="tpu_custom_call" | custom-call | tf_op jit(solution)/shard_map/pallas_call | solution.py:81
  86.6 0.8 reduce_sum.28
  87.3 0.1 add_rsqrt_fusion.1
  87.4 40.8 %reduce-scatter.2.cloned.1.call-done = bf16[32,8192]{1,0:T(8,128)(2,1)} async-done(((bf16[256,8192]{1,0:T(8,128)(2,1)}), bf16[32,8192]{1,0:T(8,128)(2,1)}) %reduce-scatter.2.cloned.1.call-update) | async-done | bytes 524304 | tf_op jit(solution)/shard_map/reduce_scatter | solution.py:397
  128.2 1.2 convert_multiply_fusion
  129.4 0.1 slice_bitcast_fusion.1
  129.7 0.6 copy.37
  130.3 1.9 copy.41
  132.2 2.2 multiply_bitcast_fusion
  134.4 33.2 %shard_map.187 = (f32[32,16,128,128]{3,2,1,0:T(8,128)}, f32[32,16,128]{2,1,0:T(8,128)S(1)}) custom-call(f32[32,16,128,128]{3,2,1,0:T(8,128)} %old_ref.1, f32[32,128,16]{2,1,0:T(8,128)S(1)} %get-tuple-element.11.forget_ref, f32[32,128,16]{2,1,0:T(8,128)S(1)} %get-tuple-element.10.query_ref, f32[32,16,128]{2,1,0:T(8,128)S(1)} %bitcast.48), custom_call_target="tpu_custom_call" | custom-call | flops 41943040 | bytes 67108864 | tf_op jit(solution)/shard_map/pallas_call | solution.py:338
  167.6 0.1 multiply_reduce_fusion
  167.8 0.1 fusion.11
  167.9 0.7 copy.48
  168.6 16.7 %shard_map.188 = bf16[8,32,2048]{2,1,0:T(8,128)(2,1)} custom-call(bf16[32,2048]{1,0:T(8,128)(2,1)} %bitcast.52), custom_call_target="tpu_custom_call" | custom-call | tf_op jit(solution)/shard_map/pallas_call | solution.py:81
  185.4 3.3 %fusion.own_ref = bf16[256,512]{1,0:T(8,128)(2,1)} fusion(bf16[256,2048]{1,0:T(8,128)(2,1)} %bitcast.51, bf16[2048,512]{1,0:T(8,128)(2,1)} %param.31, bf16[256,512]{1,0:T(8,128)(2,1)S(1)} %copy-done), kind=kOutput, calls=%fused_computation.8 | convolution fusion | flops 537264128 | bytes 3670016 | tf_op jit(solution)/shard_map/dot_general | solution.py:432
  188.7 54.2 %shard_map.189 = bf16[256,512]{1,0:T(8,128)(2,1)} custom-call(bf16[256,512]{1,0:T(8,128)(2,1)} %fusion.own_ref, f32[8,1,512]{2,1,0:T(1,128)} %bitcast.56, bf16[4096,1408]{1,0:T(8,128)(2,1)} %gate_hbm.3, bf16[4096,1408]{1,0:T(8,128)(2,1)} %up_hbm.3, bf16[1408,4096]{1,0:T(8,128)(2,1)} %down_hbm.3), custom_call_target="tpu_custom_call" | custom-call | tf_op jit(solution)/shard_map/pallas_call | solution.py:285
  242.9 1.7 copy.50
  (17 shorter events, 0.3 us)
Async XLA Ops:
  7.2 121.0 %reduce-scatter.2.cloned.1.call-start = ((), (), s32[]{:S(2)}) async-start(), calls=%async_computation.1 | async-start | bytes 4718592 | tf_op jit(solution)/shard_map/reduce_scatter | solution.py:397
  64.5 2.6 %copy-start = (bf16[256,512]{1,0:T(8,128)(2,1)S(1)}, bf16[256,512]{1,0:T(8,128)(2,1)}, u32[]{:S(2)}) copy-start(bf16[256,512]{1,0:T(8,128)(2,1)} %shard_map.185) | copy-start | bytes 786436
  64.5 2.6 %copy-start.1 = (bf16[512,2048]{1,0:T(8,128)(2,1)S(1)}, bf16[512,2048]{1,0:T(8,128)(2,1)}, u32[]{:S(2)}) copy-start(bf16[512,2048]{1,0:T(8,128)(2,1)} %param.27) | copy-start | bytes 6291460
  67.0 1.6 copy-start.2
  68.6 1.6 copy-start.3
  73.2 0.7 copy-start.4
  134.4 33.4 %copy-start.5 = (f32[128]{0:T(128)S(1)}, f32[128]{0:T(128)}, u32[]{:S(2)}) copy-start(f32[128]{0:T(128)} %param.30) | copy-start | bytes 1540
Sparse Core Ops, SparseCore 0:
  73.3 54.8 reduce-scatter.1
where the time goes:
time: 253 us; the launch traced here: 251 us
  Pallas kernels  172 us (68%)
  waiting for transfers between devices  40.8 us (16%)
  between operations  14.2 us (6%)
  local copies, waits for them, and re-layouts  9.09 us (4%)
  matrix products  8 us (3%)
  other arithmetic  6.94 us (3%)
    pallas_call x2, Pallas kernels, feed_forward(): pl.pallas_call(functools.partial(block_kernel, chips), out_shape=jax.Shap...  111 us
    reduce_scatter x1, waiting for transfers between devices, per_device(): lax.psum_scatter(jnp.concatenate([jnp.dot(mix_scaled, weight_part, prefer...  40.8 us
    pallas_call x1, Pallas kernels, update_state(): pl.pallas_call(state_kernel, grid=(rows // batch,), out_shape=(jax.ShapeD...  33.2 us
    pallas_call x2, Pallas kernels, gather_rows(): pl.pallas_call(functools.partial(gather_kernel, chips), out_shape=jax.Sha...  28.5 us
  transfers between devices with their start and end apart: 1, of which 1 were waited for; matrix products, arithmetic and copies ran while one was open for 1% of the time, Pallas kernels for 5%

commit v1 on v0

v1 whole, which is shorter than its diff:
```python
import functools

import jax
import jax.numpy as jnp
from jax import lax
from jax.experimental import pallas as pl
from jax.experimental.pallas import tpu as pltpu
from jax.sharding import PartitionSpec as P

epsilon = 1e-06
MESH = pl.DeviceIdType.MESH
VMEM_LIMIT = 63 * 1024 * 1024
LANES = 128


def remote(src, dst, send_sem, recv_sem, kv, tp):
    return pltpu.make_async_remote_copy(
        src_ref=src,
        dst_ref=dst,
        send_sem=send_sem,
        recv_sem=recv_sem,
        device_id={"kv": kv, "tp": tp},
        device_id_type=MESH,
    )


def greet_all(me, core, chips):
    barrier = pltpu.get_barrier_semaphore()
    pl.semaphore_signal(
        barrier, inc=1, device_id={"kv": me, "tp": 1 - core}, device_id_type=MESH
    )
    for step in range(1, chips):
        pl.semaphore_signal(
            barrier,
            inc=1,
            device_id={"kv": lax.rem(me + step, chips), "tp": core},
            device_id_type=MESH,
        )
    pl.semaphore_wait(barrier, chips)


def greet_chain(me, core, chips):
    barrier = pltpu.get_barrier_semaphore()
    pl.semaphore_signal(
        barrier, inc=1, device_id={"kv": me, "tp": 1 - core}, device_id_type=MESH
    )

    @pl.when(me > 0)
    def _():
        pl.semaphore_signal(
            barrier, inc=1, device_id={"kv": me - 1, "tp": core}, device_id_type=MESH
        )

    @pl.when(me < chips - 1)
    def _():
        pl.semaphore_signal(
            barrier, inc=1, device_id={"kv": me + 1, "tp": core}, device_id_type=MESH
        )

    ends = jnp.where(me > 0, 1, 0) + jnp.where(me < chips - 1, 1, 0)
    pl.semaphore_wait(barrier, 1 + ends)


def block_kernel(
    chips,
    own_ref,
    gain_ref,
    gate_hbm,
    up_hbm,
    down_hbm,
    out_ref,
    gate_w,
    up_w,
    down_w,
    cols,
    gate_acc,
    up_acc,
    squares,
    hidden,
    held,
    sib_out,
    sib_in,
    chip_out,
    chip_in,
    gate_sem,
    up_sem,
    down_sem,
    local_sem,
    fwd_send,
    pass_send,
    recv_sem,
    sib_send,
    sib_recv,
    chip_send,
    chip_recv,
):
    me = lax.axis_index("kv")
    core = lax.axis_index("tp")
    mine = me * 2 + core
    last = chips - 1
    rows, width = own_ref.shape
    full_width = width * chips * 2
    half = rows // 2
    subs = (0, 1)

    def piece(sub):
        return pl.ds(sub * half, half)

    def gate_copy(j):
        at = pl.ds(pl.multiple_of(j * width, width), width)
        return pltpu.make_async_copy(gate_hbm.at[at, :], gate_w.at[j], gate_sem.at[j])

    def up_copy(j):
        at = pl.ds(pl.multiple_of(j * width, width), width)
        return pltpu.make_async_copy(up_hbm.at[at, :], up_w.at[j], up_sem.at[j])

    def down_copy(j):
        at = pl.ds(pl.multiple_of(j * width, width), width)
        return pltpu.make_async_copy(down_hbm.at[:, at], down_w.at[j], down_sem.at[j])

    local = pltpu.make_async_copy(own_ref, cols.at[mine], local_sem)
    local.start()

    def reach(step, side):
        j = me + step * (2 * side - 1)
        fits = jnp.logical_and(j >= 0, j < chips)
        return j, jnp.logical_and(fits, jnp.logical_or(step > 0, side == 0))

    def each_block(body):
        @pl.loop(0, chips)
        def _(step):
            @pl.loop(0, 4)
            def _(i):
                j, valid = reach(step, lax.rem(i, 2))
                other = lax.div(i, 2)

                @pl.when(valid)
                def _():
                    body(j * 2 + lax.rem(core + other, 2))

    def start_in(slot):
        gate_copy(slot).start()
        up_copy(slot).start()

    each_block(start_in)
    greet_chain(me, core, chips)

    def own_copy(to, tp, sem, sub):
        at = piece(sub)
        return remote(
            own_ref.at[at], cols.at[mine, at], sem, recv_sem.at[mine, sub], to, tp
        )

    def right_copy(sub):
        return own_copy(me + 1, core, fwd_send.at[me, sub], sub)

    def left_copy(sub):
        return own_copy(me - 1, core, fwd_send.at[chips, sub], sub)

    def own_pass(sub):
        return own_copy(me, 1 - core, pass_send.at[me, sub], sub)

    def slot_copy(slot, sub, sem, to, tp):
        at = piece(sub)
        return remote(
            cols.at[slot, at], cols.at[slot, at], sem, recv_sem.at[slot, sub], to, tp
        )

    def fwd_copy(j, sub):
        to = jnp.where(j < me, me + 1, me - 1)
        return slot_copy(j * 2 + core, sub, fwd_send.at[j, sub], to, core)

    def pass_copy(j, sub):
        return slot_copy(j * 2 + core, sub, pass_send.at[j, sub], me, 1 - core)

    def forwards(j):
        return jnp.logical_or(
            jnp.logical_and(j < me, me < last), jnp.logical_and(j > me, me > 0)
        )

    for sub in subs:

        @pl.when(me < last)
        def _():
            right_copy(sub).start()

        @pl.when(me > 0)
        def _():
            left_copy(sub).start()

    for sub in subs:
        own_pass(sub).start()

    def start_down(q):
        down_copy(q * 2 + 1 - core).start()
        down_copy(q * 2 + core).start()

    def far_first(body):
        @pl.loop(0, chips)
        def _(turn):
            @pl.loop(0, 2)
            def _(side):
                q, valid = reach(last - turn, side)

                @pl.when(valid)
                def _():
                    body(q)

    far_first(start_down)

    gate_acc[...] = jnp.zeros_like(gate_acc)
    up_acc[...] = jnp.zeros_like(up_acc)
    squares[...] = jnp.zeros_like(squares)
    local.wait()

    def take(j):
        block = cols[j].astype(jnp.float32)
        squares[...] += jnp.sum(block * block, axis=1, keepdims=True)
        scaled = (block * gain_ref[j]).astype(jnp.bfloat16)
        gate_copy(j).wait()
        gate_acc[...] += jnp.dot(scaled, gate_w[j], preferred_element_type=jnp.float32)
        up_copy(j).wait()
        up_acc[...] += jnp.dot(scaled, up_w[j], preferred_element_type=jnp.float32)

    @pl.loop(0, chips)
    def _(step):
        @pl.when(step > 0)
        def _():
            for sub in subs:
                for side in (0, 1):
                    j, valid = reach(step, side)

                    @pl.when(valid)
                    def _():
                        pass_copy(j, sub).wait_recv()

                        @pl.when(forwards(j))
                        def _():
                            fwd_copy(j, sub).start()

                        pass_copy(j, sub).start()

        @pl.loop(0, 4)
        def _(i):
            j, valid = reach(step, lax.rem(i, 2))
            other = lax.div(i, 2)
            slot = j * 2 + lax.rem(core + other, 2)

            @pl.when(valid)
            def _():
                @pl.when(other == 1)
                def _():
                    for sub in subs:
                        slot_copy(slot, sub, fwd_send.at[0, 0], me, 1 - core).wait_recv()

                take(slot)

    tile = 32

    @pl.loop(0, rows // tile)
    def _(i):
        at = pl.ds(pl.multiple_of(i * tile, tile), tile)
        row_scale = lax.rsqrt(squares[at, :] / full_width + epsilon)
        gate = row_scale * gate_acc[at, :]
        hidden[at, :] = (gate * jax.nn.sigmoid(gate) * (row_scale * up_acc[at, :])).astype(
            jnp.bfloat16
        )

    def branch(j):
        down_copy(j).wait()
        return 0.5 * jnp.dot(hidden[...], down_w[j], preferred_element_type=jnp.float32)

    def sib_copy(q):
        return remote(
            sib_out.at[q], sib_in.at[q], sib_send.at[q], sib_recv.at[q], me, 1 - core
        )

    def chain_copy(q, sub):
        at = piece(sub)
        to = jnp.where(q > me, me + 1, me - 1)
        slot = jnp.where(q == me - 1, chips, q)
        return remote(
            chip_out.at[q, at],
            chip_in.at[slot, at],
            chip_send.at[q, sub],
            chip_recv.at[slot, sub],
            to,
            core,
        )

    def arrived(slot, sub):
        at = piece(sub)
        remote(
            chip_in.at[slot, at],
            chip_in.at[slot, at],
            chip_send.at[0, sub],
            chip_recv.at[slot, sub],
            me,
            1 - core,
        ).wait_recv()

    def produce(q):
        sib_out[q] = branch(q * 2 + 1 - core).astype(jnp.bfloat16)
        sib_copy(q).start()
        held[q] = branch(q * 2 + core)
        first = jnp.logical_or(
            jnp.logical_and(q > me, me == 0), jnp.logical_and(q < me, me == last)
        )

        @pl.when(first)
        def _():
            sib_copy(q).wait_recv()
            for sub in subs:
                at = piece(sub)
                chip_out[q, at] = (held[q, at] + sib_in[q, at].astype(jnp.float32)).astype(
                    jnp.bfloat16
                )
                chain_copy(q, sub).start()

    far_first(produce)

    near = jnp.where(me <= last - me, 0, 1)

    @pl.loop(1, chips - 1)
    def _(turn):
        for sub in subs:

            @pl.loop(0, 2)
            def _(i):
                leftward = lax.rem(i + near, 2)
                q = jnp.where(leftward == 1, turn - (last - me), last - (turn - me))
                goes_right = jnp.logical_and(
                    jnp.logical_and(leftward == 0, me > 0),
                    jnp.logical_and(q > me, q < chips),
                )
                goes_left = jnp.logical_and(
                    jnp.logical_and(leftward == 1, me < last),
                    jnp.logical_and(q >= 0, q < me),
                )

                @pl.when(jnp.logical_or(goes_right, goes_left))
                def _():
                    if sub == 0:
                        sib_copy(q).wait_recv()
                    arrived(q, sub)
                    at = piece(sub)
                    chip_out[q, at] = (
                        held[q, at]
                        + sib_in[q, at].astype(jnp.float32)
                        + chip_in[q, at].astype(jnp.float32)
                    ).astype(jnp.bfloat16)
                    chain_copy(q, sub).start()

    sib_copy(me).wait_recv()
    for sub in subs:
        at = piece(sub)
        held[me, at] += sib_in[me, at].astype(jnp.float32)

        @pl.when(me > 0)
        def _():
            arrived(me, sub)
            held[me, at] += chip_in[me, at].astype(jnp.float32)

        @pl.when(me < last)
        def _():
            arrived(chips, sub)
            held[me, at] += chip_in[chips, at].astype(jnp.float32)

        out_ref[at] = (held[me, at] + own_ref[at].astype(jnp.float32)).astype(out_ref.dtype)

    for sub in subs:

        @pl.when(me < last)
        def _():
            right_copy(sub).wait_send()

        @pl.when(me > 0)
        def _():
            left_copy(sub).wait_send()

    @pl.loop(0, chips)
    def _(j):
        sib_copy(j).wait_send()
        for sub in subs:
            pass_copy(j, sub).wait_send()

            @pl.when(forwards(j))
            def _():
                fwd_copy(j, sub).wait_send()

            @pl.when(j != me)
            def _():
                chain_copy(j, sub).wait_send()


def feed_forward(own, gain, gate, up, down, chips, collective_id):
    rows, width = own.shape
    units = gate.shape[1]
    blocks = chips * 2
    dma = pltpu.SemaphoreType.DMA
    half_rounds = (chips, rows, width)
    return pl.pallas_call(
        functools.partial(block_kernel, chips),
        out_shape=jax.ShapeDtypeStruct((rows, width), jnp.bfloat16),
        in_specs=[pl.BlockSpec(memory_space=pltpu.VMEM)] * 2
        + [pl.BlockSpec(memory_space=pl.ANY)] * 3,
        out_specs=pl.BlockSpec(memory_space=pltpu.VMEM),
        scratch_shapes=[
            pltpu.VMEM((blocks, width, units), jnp.bfloat16),
            pltpu.VMEM((blocks, width, units), jnp.bfloat16),
            pltpu.VMEM((blocks, units, width), jnp.bfloat16),
            pltpu.VMEM((blocks, rows, width), jnp.bfloat16),
            pltpu.VMEM((rows, units), jnp.float32),
            pltpu.VMEM((rows, units), jnp.float32),
            pltpu.VMEM((rows, 1), jnp.float32),
            pltpu.VMEM((rows, units), jnp.bfloat16),
            pltpu.VMEM(half_rounds, jnp.float32),
            pltpu.VMEM(half_rounds, jnp.bfloat16),
            pltpu.VMEM(half_rounds, jnp.bfloat16),
            pltpu.VMEM(half_rounds, jnp.bfloat16),
            pltpu.VMEM((chips + 1, rows, width), jnp.bfloat16),
            dma((blocks,)),
            dma((blocks,)),
            dma((blocks,)),
            dma,
            dma((chips + 1, 2)),
            dma((chips, 2)),
            dma((blocks, 2)),
            dma((chips,)),
            dma((chips,)),
            dma((chips, 2)),
            dma((chips + 1, 2)),
        ],
        compiler_params=pltpu.CompilerParams(
            collective_id=collective_id, has_side_effects=True, vmem_limit_bytes=VMEM_LIMIT
        ),
    )(own, gain.reshape(blocks, 1, width), gate, up, down)


def picker():
    row = lax.broadcasted_iota(jnp.int32, (16, 8 * LANES), 0)
    col = lax.broadcasted_iota(jnp.int32, (16, 8 * LANES), 1)
    return (lax.rem(row, 8) == lax.div(col, LANES)).astype(jnp.bfloat16)


def spread(eight, pick):
    high = eight.astype(jnp.bfloat16).astype(jnp.float32)
    both = jnp.concatenate([high, eight - high], axis=0).astype(jnp.bfloat16)
    return lax.dot_general(
        both, pick, (((0,), (0,)), ((), ())), preferred_element_type=jnp.float32
    )


def encode(total):
    lane = lax.broadcasted_iota(jnp.int32, (total.shape[0], LANES), 1)
    high = total.astype(jnp.bfloat16).astype(jnp.float32)
    return jnp.where(lane < LANES // 2, high, total - high)


def decode(pairs):
    return jnp.sum(pairs, axis=1, keepdims=True) * (2.0 / LANES)


def mixer_kernel(
    chips,
    pieces,
    own_ref,
    gain_ref,
    floor_ref,
    head_ref,
    query_hbm,
    forget_hbm,
    input_hbm,
    outgate_hbm,
    output_hbm,
    state_hbm,
    middle_ref,
    forget_ref,
    value_ref,
    weights,
    out_w,
    state,
    scaled,
    part,
    sib_in,
    chip_out,
    chip_in,
    total,
    scale,
    pick,
    mass,
    readout,
    mix_own,
    mixed,
    update,
    weight_sem,
    out_sem,
    state_sem,
    sib_send,
    sib_recv,
    chip_send,
    chip_recv,
    mix_send,
    pass_send,
    mix_recv,
):
    me = lax.axis_index("kv")
    core = lax.axis_index("tp")
    mine = me * 2 + core
    last = chips - 1
    rows, width = own_ref.shape
    full_width = width * chips * 2
    blocks = chips * 2
    seqs = rows // blocks
    span = weights.shape[3]
    heads = state.shape[2]
    main = 4 * span
    projections = (query_hbm, forget_hbm, input_hbm, outgate_hbm)

    def weight_copy(c, p):
        at = pl.ds(pl.multiple_of(c * span, span), span)
        return pltpu.make_async_copy(
            projections[p].at[:, at], weights.at[c, p], weight_sem.at[c, p]
        )

    def state_copy(c):
        return pltpu.make_async_copy(
            state_hbm.at[:, pl.ds(c * heads, heads)], state.at[c], state_sem.at[c]
        )

    out_copy = pltpu.make_async_copy(output_hbm, out_w, out_sem)

    @pl.loop(0, pieces)
    def _(c):
        for p in range(4):
            weight_copy(c, p).start()

    @pl.loop(0, pieces)
    def _(c):
        state_copy(c).start()

    out_copy.start()
    wide = own_ref[...].astype(jnp.float32)
    scaled[...] = (wide * gain_ref[mine]).astype(jnp.bfloat16)
    part[0, :, :, main:] = (
        encode(jnp.sum(wide * wide, axis=1, keepdims=True))
        .reshape(blocks, seqs, LANES)
        .astype(jnp.bfloat16)
    )
    pick[...] = picker()
    update[...] = wide
    greet_all(me, core, chips)

    def for_width(c, body):
        @pl.when(c == 0)
        def _():
            body(main + LANES)

        @pl.when(c > 0)
        def _():
            body(main)

    def sib_copy(c, q, size):
        at = pl.ds(0, size)
        return remote(
            part.at[c, q * 2 + 1 - core, :, at],
            sib_in.at[c, q, :, at],
            sib_send.at[c, q],
            sib_recv.at[c, q],
            me,
            1 - core,
        )

    def chain_copy(c, q, size):
        at = pl.ds(0, size)
        to = jnp.where(q > me, me + 1, me - 1)
        slot = jnp.where(q == me - 1, chips, q)
        return remote(
            chip_out.at[c, q, :, at],
            chip_in.at[c, slot, :, at],
            chip_send.at[c, q],
            chip_recv.at[c, slot],
            to,
            core,
        )

    def arrived(c, slot, size):
        at = pl.ds(0, size)
        remote(
            chip_in.at[c, slot, :, at],
            chip_in.at[c, slot, :, at],
            chip_send.at[c, 0],
            chip_recv.at[c, slot],
            me,
            1 - core,
        ).wait_recv()

    def local_sum(c, q, at):
        return part[c, q * 2 + core, :, at].astype(jnp.float32) + sib_in[c, q, :, at].astype(
            jnp.float32
        )

    def pass_on(c, q, upstream):
        def body(size):
            sib_copy(c, q, size).wait_recv()
            if upstream:
                arrived(c, q, size)

            def summed(at):
                here = local_sum(c, q, at)
                if upstream:
                    here = here + chip_in[c, q, :, at].astype(jnp.float32)
                return here

            chip_out[c, q, :, :main] = summed(slice(0, main)).astype(jnp.bfloat16)
            if size > main:
                at = slice(main, main + LANES)
                chip_out[c, q, :, at] = encode(decode(summed(at))).astype(jnp.bfloat16)
            chain_copy(c, q, size).start()

        for_width(c, body)

    @pl.loop(0, pieces)
    def _(c):
        for p in range(4):
            weight_copy(c, p).wait()
            part[c, :, :, p * span : (p + 1) * span] = (
                jnp.dot(scaled[...], weights[c, p], preferred_element_type=jnp.float32)
                .reshape(blocks, seqs, span)
                .astype(jnp.bfloat16)
            )

        @pl.loop(0, chips)
        def _(turn):
            q = jnp.where(me * 2 < chips, last - turn, turn)
            for_width(c, lambda size: sib_copy(c, q, size).start())

        @pl.loop(0, chips - 1)
        def _(turn):
            @pl.when(me == 0)
            def _():
                pass_on(c, last - turn, False)

            @pl.when(me == last)
            def _():
                pass_on(c, turn, False)

    near = jnp.where(me <= last - me, 0, 1)

    def mix_copy(c, to):
        return remote(
            mix_own.at[c],
            mixed.at[c, mine],
            mix_send.at[c, to],
            mix_recv.at[c, mine],
            to,
            core,
        )

    def own_pass(c):
        return remote(
            mix_own.at[c],
            mixed.at[c, mine],
            mix_send.at[c, me],
            mix_recv.at[c, mine],
            me,
            1 - core,
        )

    def pass_copy(c, slot, sem):
        return remote(
            mixed.at[c, slot], mixed.at[c, slot], sem, mix_recv.at[c, slot], me, 1 - core
        )

    def finish(c):
        def gather_total(size):
            sib_copy(c, me, size).wait_recv()
            at = slice(0, size)
            total[:, at] = local_sum(c, me, at)

            @pl.when(me > 0)
            def _():
                arrived(c, me, size)
                total[:, at] += chip_in[c, me, :, at].astype(jnp.float32)

            @pl.when(me < last)
            def _():
                arrived(c, chips, size)
                total[:, at] += chip_in[c, chips, :, at].astype(jnp.float32)

        for_width(c, gather_total)

        @pl.when(c == 0)
        def _():
            squares = decode(total[:, main : main + LANES])
            scale[...] = jnp.broadcast_to(
                lax.rsqrt(squares / full_width + epsilon), scale.shape
            )

        row_scale = scale[:, 0:1]
        query = row_scale * total[:, 0:span]
        query = query * jax.nn.sigmoid(query)
        floor = floor_ref[c]
        forget = floor + (1.0 - floor) * jax.nn.sigmoid(row_scale * total[:, span : 2 * span])
        value = row_scale * total[:, 2 * span : 3 * span]
        forget_ref[c] = forget
        value_ref[c] = value
        mass[...] = query * forget
        rest = query - query * forget
        state_copy(c).wait()

        @pl.loop(0, seqs // 8)
        def _(octet):
            at = pl.ds(pl.multiple_of(octet * 8, 8), 8)
            for h in range(heads):
                lanes = slice(h * LANES, (h + 1) * LANES)
                wide_mass = spread(mass[at, lanes], pick[...])
                lines = []
                for i in range(8):
                    old = state[c, octet * 8 + i, h]
                    lines.append(
                        jnp.sum(
                            old * wide_mass[:, i * LANES : (i + 1) * LANES],
                            axis=0,
                            keepdims=True,
                        )
                    )
                readout[at, lanes] = jnp.concatenate(lines, axis=0)

        gate = row_scale * total[:, 3 * span : 4 * span]
        gate = gate * jax.nn.sigmoid(gate)
        for h in range(heads):
            lanes = slice(h * LANES, (h + 1) * LANES)
            read = readout[:, lanes] + value[:, lanes] * jnp.sum(
                rest[:, lanes], axis=1, keepdims=True
            )
            read = (
                read
                * lax.rsqrt(jnp.mean(read * read, axis=1, keepdims=True) + epsilon)
                * head_ref[...]
                * gate[:, lanes]
            )
            mix_own[c, :, lanes] = read.astype(jnp.bfloat16)

        @pl.loop(1, chips)
        def _(step):
            mix_copy(c, lax.rem(me + step, chips)).start()

        own_pass(c).start()
        mixed[c, mine] = mix_own[c]

    def gather(c):
        @pl.loop(1, chips)
        def _(step):
            q = lax.rem(me + step, chips)
            pass_copy(c, q * 2 + core, mix_send.at[c, 0]).wait_recv()
            pass_copy(c, q * 2 + core, pass_send.at[c, q]).start()

        @pl.loop(0, chips)
        def _(q):
            pass_copy(c, q * 2 + 1 - core, mix_send.at[c, 0]).wait_recv()

        @pl.when(c == 0)
        def _():
            out_copy.wait()

        every = mixed[c].astype(jnp.float32).reshape(rows, span).astype(jnp.bfloat16)
        at = pl.ds(pl.multiple_of(c * span, span), span)
        update[...] += jnp.dot(every, out_w[at, :], preferred_element_type=jnp.float32)

    @pl.loop(0, pieces)
    def _(c):
        @pl.loop(1, chips - 1)
        def _(turn):
            @pl.loop(0, 2)
            def _(i):
                leftward = lax.rem(i + near, 2)
                q = jnp.where(leftward == 1, turn - (last - me), last - (turn - me))
                goes_right = jnp.logical_and(
                    jnp.logical_and(leftward == 0, me > 0),
                    jnp.logical_and(q > me, q < chips),
                )
                goes_left = jnp.logical_and(
                    jnp.logical_and(leftward == 1, me < last),
                    jnp.logical_and(q >= 0, q < me),
                )

                @pl.when(jnp.logical_or(goes_right, goes_left))
                def _():
                    pass_on(c, q, True)

        finish(c)

        @pl.when(c > 0)
        def _():
            gather(c - 1)

    gather(pieces - 1)
    middle_ref[...] = update[...].astype(middle_ref.dtype)

    @pl.loop(0, pieces)
    def _(c):
        own_pass(c).wait_send()

        @pl.loop(0, chips)
        def _(q):
            for_width(c, lambda size: sib_copy(c, q, size).wait_send())

        @pl.loop(1, chips)
        def _(step):
            q = lax.rem(me + step, chips)
            mix_copy(c, q).wait_send()
            pass_copy(c, q * 2 + core, pass_send.at[c, q]).wait_send()
            for_width(c, lambda size: chain_copy(c, q, size).wait_send())


def mixer(own, gain, weights, output_weight, carried, floor, head_gain, chips, collective_id):
    rows, width = own.shape
    seqs, head_count, key_size, value_size = carried.shape
    blocks = chips * 2
    pieces = 4
    heads = head_count // pieces
    span = heads * key_size
    extent = 4 * span + LANES
    dma = pltpu.SemaphoreType.DMA
    vmem = pl.BlockSpec(memory_space=pltpu.VMEM)
    hbm = pl.BlockSpec(memory_space=pl.ANY)
    lines = jax.ShapeDtypeStruct((pieces, seqs, span), jnp.float32)
    return pl.pallas_call(
        functools.partial(mixer_kernel, chips, pieces),
        out_shape=(jax.ShapeDtypeStruct((rows, width), jnp.bfloat16), lines, lines),
        in_specs=[vmem] * 4 + [hbm] * 6,
        out_specs=(vmem, vmem, vmem),
        scratch_shapes=[
            pltpu.VMEM((pieces, 4, width, span), jnp.bfloat16),
            pltpu.VMEM(output_weight.shape, jnp.bfloat16),
            pltpu.VMEM((pieces, seqs, heads, key_size, value_size), jnp.float32),
            pltpu.VMEM((rows, width), jnp.bfloat16),
            pltpu.VMEM((pieces, blocks, seqs, extent), jnp.bfloat16),
            pltpu.VMEM((pieces, chips, seqs, extent), jnp.bfloat16),
            pltpu.VMEM((pieces, chips, seqs, extent), jnp.bfloat16),
            pltpu.VMEM((pieces, chips + 1, seqs, extent), jnp.bfloat16),
            pltpu.VMEM((seqs, extent), jnp.float32),
            pltpu.VMEM((seqs, LANES), jnp.float32),
            pltpu.VMEM((16, 8 * LANES), jnp.bfloat16),
            pltpu.VMEM((seqs, span), jnp.float32),
            pltpu.VMEM((seqs, span), jnp.float32),
            pltpu.VMEM((pieces, seqs, span), jnp.bfloat16),
            pltpu.VMEM((pieces, blocks, seqs, span), jnp.bfloat16),
            pltpu.VMEM((rows, width), jnp.float32),
            dma((pieces, 4)),
            dma,
            dma((pieces,)),
            dma((pieces, chips)),
            dma((pieces, chips)),
            dma((pieces, chips)),
            dma((pieces, chips + 1)),
            dma((pieces, chips)),
            dma((pieces, chips)),
            dma((pieces, blocks)),
        ],
        compiler_params=pltpu.CompilerParams(
            collective_id=collective_id, has_side_effects=True, vmem_limit_bytes=VMEM_LIMIT
        ),
    )(
        own,
        gain.reshape(blocks, 1, width),
        floor.reshape(pieces, 1, span),
        head_gain.reshape(1, value_size),
        *weights,
        output_weight,
        carried,
    )


def state_kernel(old_ref, forget_ref, value_ref, new_ref):
    rows, heads = old_ref.shape[:2]
    groups, _, span = forget_ref.shape
    pick = picker()
    per = span // LANES
    for h in range(heads):
        group = h // per
        lanes = slice((h % per) * LANES, (h % per + 1) * LANES)
        wide = spread(forget_ref[group, :, lanes], pick)
        for s in range(rows):
            value = value_ref[group, s : s + 1, lanes]
            new_ref[s, h] = value + wide[:, s * LANES : (s + 1) * LANES] * (old_ref[s, h] - value)


def update_state(carried, forget, value):
    rows, heads, keys, values = carried.shape
    pieces, _, span = forget.shape
    batch = 8
    cut = span // keys * (2 if pieces % 2 == 0 else 1)
    groups = cut * keys // span
    cells = rows * heads * keys * values
    lines = pl.BlockSpec((groups, batch, span), lambda i, j: (j, i, 0))
    grid = pl.BlockSpec((batch, cut, keys, values), lambda i, j: (i, j, 0, 0))
    return pl.pallas_call(
        state_kernel,
        grid=(rows // batch, heads // cut),
        out_shape=jax.ShapeDtypeStruct(carried.shape, jnp.float32),
        in_specs=[grid, lines, lines],
        out_specs=grid,
        compiler_params=pltpu.CompilerParams(vmem_limit_bytes=32 * 1024 * 1024),
        cost_estimate=pl.CostEstimate(
            flops=20 * cells, bytes_accessed=8 * cells, transcendentals=0
        ),
    )(carried, forget, value)


def per_device(
    tokens,
    carried_state,
    first_gain,
    first_gate,
    first_up,
    first_down,
    mix_gain,
    query_weight,
    forget_weight,
    input_weight,
    outgate_weight,
    forget_floor,
    head_gain,
    output_weight,
    second_gain,
    second_gate,
    second_up,
    second_down,
):
    chips = lax.axis_size("kv")
    mixer_share = feed_forward(tokens, first_gain, first_gate, first_up, first_down, chips, 0)
    middle, forget, value = mixer(
        mixer_share,
        mix_gain,
        (query_weight, forget_weight, input_weight, outgate_weight),
        output_weight,
        carried_state,
        forget_floor,
        head_gain,
        chips,
        1,
    )
    next_state = update_state(carried_state, forget, value)
    layer_out = feed_forward(middle, second_gain, second_gate, second_up, second_down, chips, 2)
    return (layer_out, next_state)


def solution(mesh):
    in_specs = (
        P("dp", ("kv", "tp")),
        P(("dp", "kv", "tp"), None, None, None),
        P(),
        P(None, ("kv", "tp")),
        P(None, ("kv", "tp")),
        P(("kv", "tp"), None),
        P(),
        P(("kv", "tp"), None),
        P(("kv", "tp"), None),
        P(("kv", "tp"), None),
        P(("kv", "tp"), None),
        P(),
        P(),
        P(None, ("kv", "tp")),
        P(),
        P(None, ("kv", "tp")),
        P(None, ("kv", "tp")),
        P(("kv", "tp"), None),
    )
    out_specs = (P("dp", ("kv", "tp")), P(("dp", "kv", "tp"), None, None, None))
    return jax.shard_map(
        per_device, mesh=mesh, in_specs=in_specs, out_specs=out_specs, check_vma=False
    )
```

time: 253 us -> 201 us (0.79)
  waiting for transfers between devices: 40.8 us -> 0 us
  Pallas kernels: 172 us -> 199 us
  between operations: 14.2 us -> 0.7 us
  local copies, waits for them, and re-layouts: 9.09 us -> 0.72 us
  matrix products: 8 us -> 0 us
  other arithmetic: 6.94 us -> 0 us
    reduce_scatter x1 -> x0, waiting for transfers between devices: 40.8 us -> none  [per_device(): lax.psum_scatter(jnp.concatenate([jnp.dot(mix_scaled, weight_part, prefer...]
    pallas_call x3 -> x2, Pallas kernels: 61.7 us -> 101 us  [the longest x1 77 us: mixer(): pl.pallas_call(functools.partial(mixer_kernel, chips, pieces), out_shape=...]
    pallas_call x2, Pallas kernels: 111 us -> 98.2 us  [feed_forward(): pl.pallas_call(functools.partial(block_kernel, chips), out_shape=jax.Shap...]
    dot_general x5 -> x0, matrix products: 8 us -> none  [the longest x4 4.67 us: per_device(): jnp.dot(mix_scaled, weight_part, preferred_element_type=jnp.float32)]
    unnamed x18 -> x7, local copies, waits for them, and re-layouts: 4.98 us -> 0.72 us
  transfers between devices with their start and end apart: 1 -> 0, of which waited for: 1 -> 0; matrix products, arithmetic and copies ran while one was open for 1% -> 0% of each run, Pallas kernels for 5% -> 0%
where the time goes in v1:
time: 201 us
  Pallas kernels  199 us (99%)
    pallas_call x2, Pallas kernels, feed_forward(): pl.pallas_call(functools.partial(block_kernel, chips), out_shape=jax.Shap...  98.2 us
    pallas_call x1, Pallas kernels, mixer(): pl.pallas_call(functools.partial(mixer_kernel, chips, pieces), out_shape=...  77 us
    pallas_call x1, Pallas kernels, update_state(): pl.pallas_call(state_kernel, grid=(rows // batch, heads // cut), out_shap...  24.2 us

profile of v1, /device:TPU:0, one launch (start us, length us, event | category | flops | bytes accessed | tf_op | source)
XLA Modules:
  0.0 200.8 jit_solution(16659868059144263963)
XLA Ops:
  0.6 49.4 %shard_map.185.own_ref = bf16[256,512]{1,0:T(8,128)(2,1)} custom-call(bf16[256,512]{1,0:T(8,128)(2,1)} %own_ref.1, f32[8,1,512]{2,1,0:T(1,128)} %bitcast.5, bf16[4096,1408]{1,0:T(8,128)(2,1)} %gate_hbm.2, bf16[4096,1408]{1,0:T(8,128)(2,1)} %up_hbm.2, bf16[1408,4096]{1,0:T(8,128)(2,1)} %down_hbm.2), custom_call_target="tpu_custom_call" | custom-call | tf_op jit(solution)/shard_map/pallas_call | solution.py:402
  50.1 77.0 %shard_map.186 = (bf16[256,512]{1,0:T(8,128)(2,1)}, f32[4,32,512]{2,1,0:T(8,128)}, f32[4,32,512]{2,1,0:T(8,128)}) custom-call(bf16[256,512]{1,0:T(8,128)(2,1)} %shard_map.185.own_ref, f32[8,1,512]{2,1,0:T(1,128)} %bitcast.6, f32[4,1,512]{2,1,0:T(1,128)} %bitcast.8, f32[1,128]{1,0:T(1,128)} %bitcast.9, bf16[512,2048]{1,0:T(8,128)(2,1)} %query_hbm.1, ...), custom_call_target="tpu_custom_call" | custom-call | tf_op jit(solution)/shard_map/pallas_call | solution.py:829
  127.1 0.0 copy-start
  127.1 0.0 copy-start.1
  127.1 48.7 %shard_map.187 = bf16[256,512]{1,0:T(8,128)(2,1)} custom-call(bf16[256,512]{1,0:T(8,128)(2,1)} %get-tuple-element.5.own_ref, f32[8,1,512]{2,1,0:T(1,128)} %bitcast.7, bf16[4096,1408]{1,0:T(8,128)(2,1)} %gate_hbm.3, bf16[4096,1408]{1,0:T(8,128)(2,1)} %up_hbm.3, bf16[1408,4096]{1,0:T(8,128)(2,1)} %down_hbm.3), custom_call_target="tpu_custom_call" | custom-call | tf_op jit(solution)/shard_map/pallas_call | solution.py:402
  175.8 0.0 copy-done
  175.9 0.0 copy-done.1
  175.9 0.0 copy-start.2
  175.9 24.2 %shard_map.188 = f32[32,16,128,128]{3,2,1,0:T(8,128)} custom-call(f32[32,16,128,128]{3,2,1,0:T(8,128)} %old_ref.1, f32[4,32,512]{2,1,0:T(8,128)S(1)} %copy-done, f32[4,32,512]{2,1,0:T(8,128)S(1)} %copy-done.1), custom_call_target="tpu_custom_call" | custom-call | flops 167772160 | bytes 67108864 | tf_op jit(solution)/shard_map/pallas_call | solution.py:899
  200.1 0.0 copy-done.2
  200.1 0.7 copy.21
Async XLA Ops:
  127.1 48.8 %copy-start = (f32[4,32,512]{2,1,0:T(8,128)S(1)}, f32[4,32,512]{2,1,0:T(8,128)}, u32[]{:S(2)}) copy-start(f32[4,32,512]{2,1,0:T(8,128)} %get-tuple-element.6.forget_ref) | copy-start | bytes 786436
  127.1 48.8 %copy-start.1 = (f32[4,32,512]{2,1,0:T(8,128)S(1)}, f32[4,32,512]{2,1,0:T(8,128)}, u32[]{:S(2)}) copy-start(f32[4,32,512]{2,1,0:T(8,128)} %get-tuple-element.7.value_ref) | copy-start | bytes 786436
  175.9 24.2 %copy-start.2 = (bf16[256,512]{1,0:T(8,128)(2,1)S(1)}, bf16[256,512]{1,0:T(8,128)(2,1)}, u32[]{:S(2)}) copy-start(bf16[256,512]{1,0:T(8,128)(2,1)} %shard_map.187) | copy-start | bytes 786436

commit v2 on v1

--- a/solution.py
+++ b/solution.py
@@ -11,6 +11,7 @@
 MESH = pl.DeviceIdType.MESH
 VMEM_LIMIT = 63 * 1024 * 1024
 LANES = 128
+CUT = 4
 
 
 def remote(src, dst, send_sem, recv_sem, kv, tp):
@@ -63,8 +64,8 @@
 
 def block_kernel(
     chips,
-    own_ref,
-    gain_ref,
+    own_hbm,
+    gain_hbm,
     gate_hbm,
     up_hbm,
     down_hbm,
@@ -73,6 +74,7 @@
     up_w,
     down_w,
     cols,
+    gain_ref,
     gate_acc,
     up_acc,
     squares,
@@ -86,6 +88,7 @@
     up_sem,
     down_sem,
     local_sem,
+    gain_sem,
     fwd_send,
     pass_send,
     recv_sem,
@@ -98,7 +101,7 @@
     core = lax.axis_index("tp")
     mine = me * 2 + core
     last = chips - 1
-    rows, width = own_ref.shape
+    rows, width = own_hbm.shape
     full_width = width * chips * 2
     half = rows // 2
     subs = (0, 1)
@@ -118,8 +121,11 @@
         at = pl.ds(pl.multiple_of(j * width, width), width)
         return pltpu.make_async_copy(down_hbm.at[:, at], down_w.at[j], down_sem.at[j])
 
-    local = pltpu.make_async_copy(own_ref, cols.at[mine], local_sem)
+    own_ref = cols.at[mine]
+    local = pltpu.make_async_copy(own_hbm, own_ref, local_sem)
     local.start()
+    gains = pltpu.make_async_copy(gain_hbm, gain_ref, gain_sem)
+    gains.start()
 
     def reach(step, side):
         j = me + step * (2 * side - 1)
@@ -144,6 +150,7 @@
 
     each_block(start_in)
     greet_chain(me, core, chips)
+    local.wait()
 
     def own_copy(to, tp, sem, sub):
         at = piece(sub)
@@ -211,7 +218,7 @@
     gate_acc[...] = jnp.zeros_like(gate_acc)
     up_acc[...] = jnp.zeros_like(up_acc)
     squares[...] = jnp.zeros_like(squares)
-    local.wait()
+    gains.wait()
 
     def take(j):
         block = cols[j].astype(jnp.float32)
@@ -366,7 +373,7 @@
             arrived(chips, sub)
             held[me, at] += chip_in[chips, at].astype(jnp.float32)
 
-        out_ref[at] = (held[me, at] + own_ref[at].astype(jnp.float32)).astype(out_ref.dtype)
+        out_ref[at] = (held[me, at] + cols[mine, at].astype(jnp.float32)).astype(out_ref.dtype)
 
     for sub in subs:
 
@@ -402,14 +409,14 @@
     return pl.pallas_call(
         functools.partial(block_kernel, chips),
         out_shape=jax.ShapeDtypeStruct((rows, width), jnp.bfloat16),
-        in_specs=[pl.BlockSpec(memory_space=pltpu.VMEM)] * 2
-        + [pl.BlockSpec(memory_space=pl.ANY)] * 3,
+        in_specs=[pl.BlockSpec(memory_space=pl.ANY)] * 5,
         out_specs=pl.BlockSpec(memory_space=pltpu.VMEM),
         scratch_shapes=[
             pltpu.VMEM((blocks, width, units), jnp.bfloat16),
             pltpu.VMEM((blocks, width, units), jnp.bfloat16),
             pltpu.VMEM((blocks, units, width), jnp.bfloat16),
             pltpu.VMEM((blocks, rows, width), jnp.bfloat16),
+            pltpu.VMEM((blocks, 1, width), jnp.float32),
             pltpu.VMEM((rows, units), jnp.float32),
             pltpu.VMEM((rows, units), jnp.float32),
             pltpu.VMEM((rows, 1), jnp.float32),
@@ -423,6 +430,7 @@
             dma((blocks,)),
             dma((blocks,)),
             dma,
+            dma,
             dma((chips + 1, 2)),
             dma((chips, 2)),
             dma((blocks, 2)),
@@ -464,10 +472,10 @@
 def mixer_kernel(
     chips,
     pieces,
-    own_ref,
-    gain_ref,
-    floor_ref,
-    head_ref,
+    own_hbm,
+    gain_hbm,
+    floor_hbm,
+    head_hbm,
     query_hbm,
     forget_hbm,
     input_hbm,
@@ -477,6 +485,10 @@
     middle_ref,
     forget_ref,
     value_ref,
+    own_ref,
+    gain_ref,
+    floor_ref,
+    head_ref,
     weights,
     out_w,
     state,
@@ -493,6 +505,7 @@
     mix_own,
     mixed,
     update,
+    small_sem,
     weight_sem,
     out_sem,
     state_sem,
@@ -508,7 +521,7 @@
     core = lax.axis_index("tp")
     mine = me * 2 + core
     last = chips - 1
-    rows, width = own_ref.shape
+    rows, width = own_hbm.shape
     full_width = width * chips * 2
     blocks = chips * 2
     seqs = rows // blocks
@@ -529,6 +542,17 @@
         )
 
     out_copy = pltpu.make_async_copy(output_hbm, out_w, out_sem)
+    small = (
+        (own_hbm, own_ref),
+        (gain_hbm.at[mine], gain_ref),
+        (floor_hbm, floor_ref),
+        (head_hbm, head_ref),
+    )
+    small = [
+        pltpu.make_async_copy(src, dst, small_sem.at[i]) for i, (src, dst) in enumerate(small)
+    ]
+    for copy in small:
+        copy.start()
 
     @pl.loop(0, pieces)
     def _(c):
@@ -540,16 +564,18 @@
         state_copy(c).start()
 
     out_copy.start()
+    pick[...] = picker()
+    greet_all(me, core, chips)
+    for copy in small:
+        copy.wait()
     wide = own_ref[...].astype(jnp.float32)
-    scaled[...] = (wide * gain_ref[mine]).astype(jnp.bfloat16)
+    scaled[...] = (wide * gain_ref[...]).astype(jnp.bfloat16)
     part[0, :, :, main:] = (
         encode(jnp.sum(wide * wide, axis=1, keepdims=True))
         .reshape(blocks, seqs, LANES)
         .astype(jnp.bfloat16)
     )
-    pick[...] = picker()
     update[...] = wide
-    greet_all(me, core, chips)
 
     def for_width(c, body):
         @pl.when(c == 0)
@@ -768,8 +794,7 @@
         at = pl.ds(pl.multiple_of(c * span, span), span)
         update[...] += jnp.dot(every, out_w[at, :], preferred_element_type=jnp.float32)
 
-    @pl.loop(0, pieces)
-    def _(c):
+    def relay(c):
         @pl.loop(1, chips - 1)
         def _(turn):
             @pl.loop(0, 2)
@@ -789,6 +814,14 @@
                 def _():
                     pass_on(c, q, True)
 
+    relay(0)
+
+    @pl.loop(0, pieces)
+    def _(c):
+        @pl.when(c < pieces - 1)
+        def _():
+            relay(c + 1)
+
         finish(c)
 
         @pl.when(c > 0)
@@ -818,7 +851,7 @@
     rows, width = own.shape
     seqs, head_count, key_size, value_size = carried.shape
     blocks = chips * 2
-    pieces = 4
+    pieces = 2
     heads = head_count // pieces
     span = heads * key_size
     extent = 4 * span + LANES
@@ -829,9 +862,13 @@
     return pl.pallas_call(
         functools.partial(mixer_kernel, chips, pieces),
         out_shape=(jax.ShapeDtypeStruct((rows, width), jnp.bfloat16), lines, lines),
-        in_specs=[vmem] * 4 + [hbm] * 6,
+        in_specs=[hbm] * 10,
         out_specs=(vmem, vmem, vmem),
         scratch_shapes=[
+            pltpu.VMEM((rows, width), jnp.bfloat16),
+            pltpu.VMEM((1, width), jnp.float32),
+            pltpu.VMEM((pieces, 1, span), jnp.float32),
+            pltpu.VMEM((1, value_size), jnp.float32),
             pltpu.VMEM((pieces, 4, width, span), jnp.bfloat16),
             pltpu.VMEM(output_weight.shape, jnp.bfloat16),
             pltpu.VMEM((pieces, seqs, heads, key_size, value_size), jnp.float32),
@@ -848,6 +885,7 @@
             pltpu.VMEM((pieces, seqs, span), jnp.bfloat16),
             pltpu.VMEM((pieces, blocks, seqs, span), jnp.bfloat16),
             pltpu.VMEM((rows, width), jnp.float32),
+            dma((4,)),
             dma((pieces, 4)),
             dma,
             dma((pieces,)),
@@ -875,15 +913,12 @@
 
 def state_kernel(old_ref, forget_ref, value_ref, new_ref):
     rows, heads = old_ref.shape[:2]
-    groups, _, span = forget_ref.shape
     pick = picker()
-    per = span // LANES
     for h in range(heads):
-        group = h // per
-        lanes = slice((h % per) * LANES, (h % per + 1) * LANES)
-        wide = spread(forget_ref[group, :, lanes], pick)
+        lanes = slice(h * LANES, (h + 1) * LANES)
+        wide = spread(forget_ref[0, :, lanes], pick)
         for s in range(rows):
-            value = value_ref[group, s : s + 1, lanes]
+            value = value_ref[0, s : s + 1, lanes]
             new_ref[s, h] = value + wide[:, s * LANES : (s + 1) * LANES] * (old_ref[s, h] - value)
 
 
@@ -891,10 +926,10 @@
     rows, heads, keys, values = carried.shape
     pieces, _, span = forget.shape
     batch = 8
-    cut = span // keys * (2 if pieces % 2 == 0 else 1)
-    groups = cut * keys // span
+    cut = min(CUT, span // keys)
+    inner = span // keys // cut
     cells = rows * heads * keys * values
-    lines = pl.BlockSpec((groups, batch, span), lambda i, j: (j, i, 0))
+    lines = pl.BlockSpec((1, batch, cut * keys), lambda i, j: (j // inner, i, j % inner))
     grid = pl.BlockSpec((batch, cut, keys, values), lambda i, j: (i, j, 0, 0))
     return pl.pallas_call(
         state_kernel,

time: 201 us -> 188 us (0.935)
  Pallas kernels: 199 us -> 187 us
    pallas_call x1, Pallas kernels: 77 us -> 58.7 us  [mixer(): pl.pallas_call(functools.partial(mixer_kernel, chips, pieces), out_shape=...]
    pallas_call x1, Pallas kernels: 24.2 us -> 29.5 us  [update_state(): pl.pallas_call(state_kernel, grid=(rows // batch, heads // cut), out_shap...]
where the time goes in v2:
time: 188 us
  Pallas kernels  187 us (99%)
    pallas_call x2, Pallas kernels, feed_forward(): pl.pallas_call(functools.partial(block_kernel, chips), out_shape=jax.Shap...  98.5 us
    pallas_call x1, Pallas kernels, mixer(): pl.pallas_call(functools.partial(mixer_kernel, chips, pieces), out_shape=...  58.7 us
    pallas_call x1, Pallas kernels, update_state(): pl.pallas_call(state_kernel, grid=(rows // batch, heads // cut), out_shap...  29.5 us

profile of v2, /device:TPU:0, one launch (start us, length us, event | category | flops | bytes accessed | tf_op | source)
XLA Modules:
  0.0 188.1 jit_solution(4815152485494779726)
XLA Ops:
  0.6 48.5 %shard_map.185.own_hbm = bf16[256,512]{1,0:T(8,128)(2,1)} custom-call(bf16[256,512]{1,0:T(8,128)(2,1)} %own_hbm.1, f32[8,1,512]{2,1,0:T(1,128)} %bitcast.5, bf16[4096,1408]{1,0:T(8,128)(2,1)} %gate_hbm.2, bf16[4096,1408]{1,0:T(8,128)(2,1)} %up_hbm.2, bf16[1408,4096]{1,0:T(8,128)(2,1)} %down_hbm.2), custom_call_target="tpu_custom_call" | custom-call | tf_op jit(solution)/shard_map/pallas_call | solution.py:409
  49.1 58.7 %shard_map.186 = (bf16[256,512]{1,0:T(8,128)(2,1)}, f32[2,32,1024]{2,1,0:T(8,128)}, f32[2,32,1024]{2,1,0:T(8,128)}) custom-call(bf16[256,512]{1,0:T(8,128)(2,1)} %shard_map.185.own_hbm, f32[8,1,512]{2,1,0:T(1,128)} %bitcast.6, f32[2,1,1024]{2,1,0:T(1,128)} %bitcast.8, f32[1,128]{1,0:T(1,128)} %bitcast.9, bf16[512,2048]{1,0:T(8,128)(2,1)} %query_hbm.1, ...), custom_call_target="tpu_custom_call" | custom-call | tf_op jit(solution)/shard_map/pallas_call | solution.py:862
  107.8 0.0 copy-start
  107.8 0.0 copy-start.1
  107.8 50.0 %shard_map.187 = bf16[256,512]{1,0:T(8,128)(2,1)} custom-call(bf16[256,512]{1,0:T(8,128)(2,1)} %get-tuple-element.5.own_hbm, f32[8,1,512]{2,1,0:T(1,128)} %bitcast.7, bf16[4096,1408]{1,0:T(8,128)(2,1)} %gate_hbm.3, bf16[4096,1408]{1,0:T(8,128)(2,1)} %up_hbm.3, bf16[1408,4096]{1,0:T(8,128)(2,1)} %down_hbm.3), custom_call_target="tpu_custom_call" | custom-call | tf_op jit(solution)/shard_map/pallas_call | solution.py:409
  157.8 0.0 copy-done
  157.9 0.0 copy-done.1
  157.9 0.0 copy-start.2
  157.9 29.5 %shard_map.188 = f32[32,16,128,128]{3,2,1,0:T(8,128)} custom-call(f32[32,16,128,128]{3,2,1,0:T(8,128)} %old_ref.1, f32[2,32,1024]{2,1,0:T(8,128)S(1)} %copy-done, f32[2,32,1024]{2,1,0:T(8,128)S(1)} %copy-done.1), custom_call_target="tpu_custom_call" | custom-call | flops 167772160 | bytes 67108864 | tf_op jit(solution)/shard_map/pallas_call | solution.py:934
  187.4 0.0 copy-done.2
  187.4 0.7 copy.21
Async XLA Ops:
  107.8 50.1 %copy-start = (f32[2,32,1024]{2,1,0:T(8,128)S(1)}, f32[2,32,1024]{2,1,0:T(8,128)}, u32[]{:S(2)}) copy-start(f32[2,32,1024]{2,1,0:T(8,128)} %get-tuple-element.6.forget_ref) | copy-start | bytes 786436
  107.8 50.1 %copy-start.1 = (f32[2,32,1024]{2,1,0:T(8,128)S(1)}, f32[2,32,1024]{2,1,0:T(8,128)}, u32[]{:S(2)}) copy-start(f32[2,32,1024]{2,1,0:T(8,128)} %get-tuple-element.7.value_ref) | copy-start | bytes 786436
  157.9 29.5 %copy-start.2 = (bf16[256,512]{1,0:T(8,128)(2,1)S(1)}, bf16[256,512]{1,0:T(8,128)(2,1)}, u32[]{:S(2)}) copy-start(bf16[256,512]{1,0:T(8,128)(2,1)} %shard_map.187) | copy-start | bytes 786436

commit v3 on v2

--- a/solution.py
+++ b/solution.py
@@ -10,8 +10,8 @@
 epsilon = 1e-06
 MESH = pl.DeviceIdType.MESH
 VMEM_LIMIT = 63 * 1024 * 1024
+MIXER_LIMIT = 29 * 1024 * 1024
 LANES = 128
-CUT = 4
 
 
 def remote(src, dst, send_sem, recv_sem, kv, tp):
@@ -483,15 +483,15 @@
     output_hbm,
     state_hbm,
     middle_ref,
-    forget_ref,
-    value_ref,
+    state,
     own_ref,
     gain_ref,
     floor_ref,
     head_ref,
     weights,
     out_w,
-    state,
+    forget_ref,
+    value_ref,
     scaled,
     part,
     sib_in,
@@ -526,7 +526,7 @@
     blocks = chips * 2
     seqs = rows // blocks
     span = weights.shape[3]
-    heads = state.shape[2]
+    heads = state.shape[1] // pieces
     main = 4 * span
     projections = (query_hbm, forget_hbm, input_hbm, outgate_hbm)
 
@@ -538,7 +538,9 @@
 
     def state_copy(c):
         return pltpu.make_async_copy(
-            state_hbm.at[:, pl.ds(c * heads, heads)], state.at[c], state_sem.at[c]
+            state_hbm.at[:, pl.ds(c * heads, heads)],
+            state.at[:, pl.ds(c * heads, heads)],
+            state_sem.at[c],
         )
 
     out_copy = pltpu.make_async_copy(output_hbm, out_w, out_sem)
@@ -743,7 +745,7 @@
                 wide_mass = spread(mass[at, lanes], pick[...])
                 lines = []
                 for i in range(8):
-                    old = state[c, octet * 8 + i, h]
+                    old = state[octet * 8 + i, c * heads + h]
                     lines.append(
                         jnp.sum(
                             old * wide_mass[:, i * LANES : (i + 1) * LANES],
@@ -774,6 +776,19 @@
 
         own_pass(c).start()
         mixed[c, mine] = mix_own[c]
+
+        @pl.loop(0, seqs // 8)
+        def _(octet):
+            at = pl.ds(pl.multiple_of(octet * 8, 8), 8)
+            for h in range(heads):
+                lanes = slice(h * LANES, (h + 1) * LANES)
+                wide_keep = spread(forget_ref[c, at, lanes], pick[...])
+                values = value_ref[c, at, lanes]
+                for i in range(8):
+                    line = values[i : i + 1]
+                    keep = wide_keep[:, i * LANES : (i + 1) * LANES]
+                    old = state[octet * 8 + i, c * heads + h]
+                    state[octet * 8 + i, c * heads + h] = line + keep * (old - line)
 
     def gather(c):
         @pl.loop(1, chips)
@@ -858,12 +873,14 @@
     dma = pltpu.SemaphoreType.DMA
     vmem = pl.BlockSpec(memory_space=pltpu.VMEM)
     hbm = pl.BlockSpec(memory_space=pl.ANY)
-    lines = jax.ShapeDtypeStruct((pieces, seqs, span), jnp.float32)
     return pl.pallas_call(
         functools.partial(mixer_kernel, chips, pieces),
-        out_shape=(jax.ShapeDtypeStruct((rows, width), jnp.bfloat16), lines, lines),
+        out_shape=(
+            jax.ShapeDtypeStruct((rows, width), jnp.bfloat16),
+            pltpu.VMEM(carried.shape, jnp.float32),
+        ),
         in_specs=[hbm] * 10,
-        out_specs=(vmem, vmem, vmem),
+        out_specs=(vmem, vmem),
         scratch_shapes=[
             pltpu.VMEM((rows, width), jnp.bfloat16),
             pltpu.VMEM((1, width), jnp.float32),
@@ -871,7 +888,8 @@
             pltpu.VMEM((1, value_size), jnp.float32),
             pltpu.VMEM((pieces, 4, width, span), jnp.bfloat16),
             pltpu.VMEM(output_weight.shape, jnp.bfloat16),
-            pltpu.VMEM((pieces, seqs, heads, key_size, value_size), jnp.float32),
+            pltpu.VMEM((pieces, seqs, span), jnp.float32),
+            pltpu.VMEM((pieces, seqs, span), jnp.float32),
             pltpu.VMEM((rows, width), jnp.bfloat16),
             pltpu.VMEM((pieces, blocks, seqs, extent), jnp.bfloat16),
             pltpu.VMEM((pieces, chips, seqs, extent), jnp.bfloat16),
@@ -898,7 +916,7 @@
             dma((pieces, blocks)),
         ],
         compiler_params=pltpu.CompilerParams(
-            collective_id=collective_id, has_side_effects=True, vmem_limit_bytes=VMEM_LIMIT
+            collective_id=collective_id, has_side_effects=True, vmem_limit_bytes=MIXER_LIMIT
         ),
     )(
         own,
@@ -911,37 +929,33 @@
     )
 
 
-def state_kernel(old_ref, forget_ref, value_ref, new_ref):
-    rows, heads = old_ref.shape[:2]
-    pick = picker()
-    for h in range(heads):
-        lanes = slice(h * LANES, (h + 1) * LANES)
-        wide = spread(forget_ref[0, :, lanes], pick)
-        for s in range(rows):
-            value = value_ref[0, s : s + 1, lanes]
-            new_ref[s, h] = value + wide[:, s * LANES : (s + 1) * LANES] * (old_ref[s, h] - value)
-
-
-def update_state(carried, forget, value):
-    rows, heads, keys, values = carried.shape
-    pieces, _, span = forget.shape
-    batch = 8
-    cut = min(CUT, span // keys)
-    inner = span // keys // cut
-    cells = rows * heads * keys * values
-    lines = pl.BlockSpec((1, batch, cut * keys), lambda i, j: (j // inner, i, j % inner))
-    grid = pl.BlockSpec((batch, cut, keys, values), lambda i, j: (i, j, 0, 0))
+def write_kernel(state, new_hbm, sem):
+    rows = state.shape[0]
+    chunks = sem.shape[0]
+    size = rows // chunks
+
+    def write_copy(i):
+        at = pl.ds(i * size, size)
+        return pltpu.make_async_copy(state.at[at], new_hbm.at[at], sem.at[i])
+
+    @pl.loop(0, chunks)
+    def _(i):
+        write_copy(i).start()
+
+    @pl.loop(0, chunks)
+    def _(i):
+        write_copy(i).wait()
+
+
+def write_state(state):
     return pl.pallas_call(
-        state_kernel,
-        grid=(rows // batch, heads // cut),
-        out_shape=jax.ShapeDtypeStruct(carried.shape, jnp.float32),
-        in_specs=[grid, lines, lines],
-        out_specs=grid,
-        compiler_params=pltpu.CompilerParams(vmem_limit_bytes=32 * 1024 * 1024),
-        cost_estimate=pl.CostEstimate(
-            flops=20 * cells, bytes_accessed=8 * cells, transcendentals=0
-        ),
-    )(carried, forget, value)
+        write_kernel,
+        out_shape=jax.ShapeDtypeStruct(state.shape, jnp.float32),
+        in_specs=[pl.BlockSpec(memory_space=pltpu.VMEM)],
+        out_specs=pl.BlockSpec(memory_space=pl.ANY),
+        scratch_shapes=[pltpu.SemaphoreType.DMA((8,))],
+        compiler_params=pltpu.CompilerParams(vmem_limit_bytes=4 * 1024 * 1024),
+    )(state)
 
 
 def per_device(
@@ -966,7 +980,7 @@
 ):
     chips = lax.axis_size("kv")
     mixer_share = feed_forward(tokens, first_gain, first_gate, first_up, first_down, chips, 0)
-    middle, forget, value = mixer(
+    middle, held_state = mixer(
         mixer_share,
         mix_gain,
         (query_weight, forget_weight, input_weight, outgate_weight),
@@ -977,7 +991,8 @@
         chips,
         1,
     )
-    next_state = update_state(carried_state, forget, value)
+    next_state = write_state(held_state)
+    middle, next_state = lax.optimization_barrier((middle, next_state))
     layer_out = feed_forward(middle, second_gain, second_gate, second_up, second_down, chips, 2)
     return (layer_out, next_state)
 

time: 188 us -> 171 us (0.910)
  Pallas kernels: 187 us -> 168 us
    pallas_call x1, Pallas kernels: 29.5 us -> 11 us  [write_state(): pl.pallas_call(write_kernel, out_shape=jax.ShapeDtypeStruct(state.shape,...]
    pallas_call x2, Pallas kernels: 98.5 us -> 96.2 us  [feed_forward(): pl.pallas_call(functools.partial(block_kernel, chips), out_shape=jax.Shap...]
    pallas_call x1, Pallas kernels: 58.7 us -> 60.9 us  [mixer(): pl.pallas_call(functools.partial(mixer_kernel, chips, pieces), out_shape=...]
where the time goes in v3:
time: 171 us; the launch traced here: 170 us
  Pallas kernels  168 us (98%)
    pallas_call x2, Pallas kernels, feed_forward(): pl.pallas_call(functools.partial(block_kernel, chips), out_shape=jax.Shap...  96.2 us
    pallas_call x1, Pallas kernels, mixer(): pl.pallas_call(functools.partial(mixer_kernel, chips, pieces), out_shape=...  60.9 us
    pallas_call x1, Pallas kernels, write_state(): pl.pallas_call(write_kernel, out_shape=jax.ShapeDtypeStruct(state.shape,...  11 us

profile of v3, /device:TPU:0, one launch (start us, length us, event | category | flops | bytes accessed | tf_op | source)
XLA Modules:
  0.0 170.5 jit_solution(8143080826341297105)
XLA Ops:
  0.6 48.5 %shard_map.185.own_hbm = bf16[256,512]{1,0:T(8,128)(2,1)} custom-call(bf16[256,512]{1,0:T(8,128)(2,1)} %own_hbm.1, f32[8,1,512]{2,1,0:T(1,128)} %bitcast.5, bf16[4096,1408]{1,0:T(8,128)(2,1)} %gate_hbm.2, bf16[4096,1408]{1,0:T(8,128)(2,1)} %up_hbm.2, bf16[1408,4096]{1,0:T(8,128)(2,1)} %down_hbm.2), custom_call_target="tpu_custom_call" | custom-call | tf_op jit(solution)/shard_map/pallas_call | solution.py:409
  49.1 60.9 %shard_map.186 = (bf16[256,512]{1,0:T(8,128)(2,1)}, f32[32,16,128,128]{3,2,1,0:T(8,128)S(1)}) custom-call(bf16[256,512]{1,0:T(8,128)(2,1)} %shard_map.185.own_hbm, f32[8,1,512]{2,1,0:T(1,128)} %bitcast.6, f32[2,1,1024]{2,1,0:T(1,128)} %bitcast.8, f32[1,128]{1,0:T(1,128)} %bitcast.9, bf16[512,2048]{1,0:T(8,128)(2,1)} %query_hbm.1, ...), custom_call_target="tpu_custom_call" | custom-call | tf_op jit(solution)/shard_map/pallas_call | solution.py:876
  110.0 11.0 %shard_map.187 = f32[32,16,128,128]{3,2,1,0:T(8,128)} custom-call(f32[32,16,128,128]{3,2,1,0:T(8,128)S(1)} %get-tuple-element.7.state), custom_call_target="tpu_custom_call" | custom-call | tf_op jit(solution)/shard_map/pallas_call | solution.py:951
  121.1 47.7 %shard_map.188 = bf16[256,512]{1,0:T(8,128)(2,1)} custom-call(bf16[256,512]{1,0:T(8,128)(2,1)} %get-tuple-element.8.own_hbm, f32[8,1,512]{2,1,0:T(1,128)} %bitcast.7, bf16[4096,1408]{1,0:T(8,128)(2,1)} %gate_hbm.3, bf16[4096,1408]{1,0:T(8,128)(2,1)} %up_hbm.3, bf16[1408,4096]{1,0:T(8,128)(2,1)} %down_hbm.3), custom_call_target="tpu_custom_call" | custom-call | tf_op jit(solution)/shard_map/pallas_call | solution.py:409
  168.8 1.7 copy.21
